TPU v7x, 128 devices: a whole 4x4x4 slice. The times are simulated.
128 devices in a mesh: ep: 128 (over z, y, x, core).
Axes of the slice: x: 4, y: 4, z: 4, core: 2. Of those that a mesh axis runs over, the one named last changes fastest.
Arguments:
- hidden_in: bfloat16 [256, 2048], P('ep'), may hold values from -6 to 6
- lengths: int32 [256], P('ep'), may hold values from 1 to 1024, as said below
- key_cache: bfloat16 [256, 1024, 512], P('ep'), may hold values from -30 to 30
- value_cache: bfloat16 [256, 1024, 512], P('ep'), may hold values from -6 to 6
- query_w: bfloat16 [2048, 2048], P('ep'), may hold values from -0.125 to 0.125
- key_w: bfloat16 [2048, 512], P('ep'), may hold values from -0.125 to 0.125
- value_w: bfloat16 [2048, 512], P('ep'), may hold values from -0.125 to 0.125
- out_w: bfloat16 [2048, 2048], P('ep'), may hold values from -0.125 to 0.125
- lam_heads: float32 [8], replicated, may hold values from 0.3 to 0.8
- head_gain: float32 [256], replicated, may hold values from 0.1 to 1.9
- attn_gain: float32 [2048], replicated, may hold values from 0.1 to 1.9
- moe_gain: float32 [2048], replicated, may hold values from 0.1 to 1.9
- routing: int32 [256, 6], replicated, may hold values from 0 to 127, all different within a row; in each aligned block of 256 rows (0 to 255, 256 to 511, ...) at most 24 rows name the same one
- route_weight: float32 [256, 6], replicated, may hold values from 0.1 to 0.6
- gate_w: bfloat16 [128, 2048, 512], P('ep'), may hold values from -0.125 to 0.125
- up_w: bfloat16 [128, 2048, 512], P('ep'), may hold values from -0.125 to 0.125
- down_w: bfloat16 [128, 512, 2048], P('ep'), may hold values from -0.25 to 0.25
- shared_gate: bfloat16 [2048, 512], replicated, may hold values from -0.125 to 0.125
- shared_up: bfloat16 [2048, 512], replicated, may hold values from -0.125 to 0.125
- shared_down: bfloat16 [512, 2048], replicated, may hold values from -0.25 to 0.25
Outputs:
- layer_out: bfloat16 [256, 2048], P('ep')
- key_new: bfloat16 [256, 512], P('ep')
- value_new: bfloat16 [256, 512], P('ep')
Inputs may be any that keep to these rules, and one draw needn't show every extreme that they name: `lengths`: some sequence has exactly 1024 positions in use. `routing`: each row names 6 different experts; no expert is named by more than 24 rows, a bound that some block reaches.
All inputs are finite; a program needn't handle non-finite values.
Results may differ from a plain program's by a relative error of at most 0.013.
The roundings to bfloat16 on the way count: a program that leaves them out, or rounds other values in their place, can miss the bound.
Values may be sent and summed in bfloat16 or wider, within the bound.
No kernel may reach another device: no remote copies, remote signals or barrier semaphores. Data moves between devices by JAX's collectives and lax.ppermute only.
A program may use at most 64 MiB of HBM per device.

v0:
```python
import jax
import jax.numpy as jnp
from jax import lax
from jax.sharding import Mesh
from jax.sharding import PartitionSpec as P

KV_HEADS = 2
HEAD_DIM = 128
EXP_CAP = 24
EP = ("ep_0", "ep_1", "ep_2", "ep_3")
eps_norm = 1e-06
eps_head = 1e-05
theta_base = 500000.0


def split_up(value, dim, length):
    dims = value.shape
    blocks = value.reshape(*dims[:dim], length, dims[dim] // length, *dims[dim + 1 :])
    return jnp.moveaxis(blocks, dim, 0)


def sent_and_summed(value, axis, dim):
    blocks = split_up(value, dim, lax.axis_size(axis))
    arrived = lax.all_to_all(blocks, axis, split_axis=0, concat_axis=0, tiled=True)
    return arrived.astype(jnp.float32).sum(axis=0)


def summed_rows(value, axes, dim):
    far, near = axes
    blocks = split_up(value, dim, lax.axis_size(far))
    nearer = sent_and_summed(blocks, near, dim + 1)
    arrived = lax.all_to_all(
        nearer.astype(jnp.bfloat16), far, split_axis=0, concat_axis=0, tiled=True
    )
    return arrived.astype(jnp.float32).sum(axis=0)


def rms_scale(row_block, gain_vec, epsilon):
    row_block = row_block.astype(jnp.float32)
    return (
        row_block
        * lax.rsqrt(jnp.mean(row_block * row_block, axis=-1, keepdims=True) + epsilon)
        * gain_vec
    )


def rotate(vectors, positions):
    half_width = vectors.shape[-1] // 2
    inverse = theta_base ** (-jnp.arange(half_width, dtype=jnp.float32) / half_width)
    angles = positions.astype(jnp.float32)[..., None] * inverse
    cosine, sine_part = (jnp.cos(angles), jnp.sin(angles))
    lower_half, upper_half = (vectors[..., :half_width], vectors[..., half_width:])
    return jnp.concatenate(
        [
            lower_half * cosine - upper_half * sine_part,
            lower_half * sine_part + upper_half * cosine,
        ],
        axis=-1,
    )


def attend(queries, key_new, value_new, cache_keys, cache_values, lengths, lam_heads, head_gain):
    num_seqs, kv_heads, group_size = (queries.shape[0], queries.shape[1], queries.shape[2])
    head_dim = queries.shape[-1]
    cache_len = cache_keys.shape[1]
    cache_keys = cache_keys.reshape(num_seqs, cache_len, kv_heads, 2, head_dim)
    cache_values = cache_values.reshape(num_seqs, cache_len, kv_heads, -1)
    value_new = value_new.reshape(num_seqs, kv_heads, -1)
    score_scale = head_dim ** (-0.5)
    scores = (
        jnp.einsum("skgph,sckph->skgpc", queries, cache_keys, preferred_element_type=jnp.float32)
        * score_scale
    )
    self_score = (
        jnp.einsum("skgph,skph->skgp", queries, key_new, preferred_element_type=jnp.float32)
        * score_scale
    )
    live_mask = (jnp.arange(cache_len)[None, :] < lengths[:, None])[:, None, None, None, :]
    peak = jnp.maximum(jnp.max(jnp.where(live_mask, scores, -jnp.inf), axis=-1), self_score)
    weights = jnp.where(live_mask, jnp.exp(scores - peak[..., None]), 0.0)
    self_weight = jnp.exp(self_score - peak)
    totals = jnp.sum(weights, axis=-1) + self_weight
    lambda_grid = lam_heads.reshape(kv_heads, group_size)[None]
    combined = (
        weights[:, :, :, 0] / totals[:, :, :, 0, None]
        - lambda_grid[..., None] * weights[:, :, :, 1] / totals[:, :, :, 1, None]
    ).astype(jnp.bfloat16)
    self_combined = (
        self_weight[..., 0] / totals[..., 0] - lambda_grid * self_weight[..., 1] / totals[..., 1]
    ).astype(jnp.bfloat16)
    head_out = jnp.einsum(
        "skgc,sckv->skgv", combined, cache_values, preferred_element_type=jnp.float32
    )
    head_out = (
        head_out
        + self_combined.astype(jnp.float32)[..., None]
        * value_new.astype(jnp.float32)[:, :, None, :]
    )
    return rms_scale(head_out, head_gain, eps_head).astype(jnp.bfloat16).reshape(num_seqs, -1)


def expert_rows(row_block, routed_here, gate_one, up_one, down_one):
    slot_index = jnp.cumsum(routed_here) - 1
    pick_table = (
        (slot_index[None, :] == jnp.arange(EXP_CAP)[:, None]) & (routed_here[None, :] > 0)
    ).astype(jnp.bfloat16)
    picked = jnp.dot(pick_table, row_block, preferred_element_type=jnp.float32).astype(jnp.bfloat16)
    hidden = (
        jax.nn.silu(jnp.dot(picked, gate_one, preferred_element_type=jnp.float32))
        * jnp.dot(picked, up_one, preferred_element_type=jnp.float32)
    ).astype(jnp.bfloat16)
    result = jnp.dot(hidden, down_one, preferred_element_type=jnp.float32).astype(jnp.bfloat16)
    return jnp.dot(pick_table.T, result, preferred_element_type=jnp.float32)


def on_device(
    hidden_in,
    lengths,
    key_cache,
    value_cache,
    query_w,
    key_w,
    value_w,
    out_w,
    lam_heads,
    head_gain,
    attn_gain,
    moe_gain,
    routing,
    route_weight,
    gate_w,
    up_w,
    down_w,
    shared_gate,
    shared_up,
    shared_down,
):
    devices = lax.axis_size(EP)
    device = lax.axis_index(EP)
    tok_dev = hidden_in.shape[0]
    model_width = hidden_in.shape[1]
    all_rows = lax.all_gather(hidden_in, EP, axis=0, tiled=True)
    normed = rms_scale(all_rows, attn_gain, eps_norm).astype(jnp.bfloat16)
    joined_rows = jnp.concatenate([query_w, key_w, value_w], axis=1)
    column_block = lax.all_to_all(joined_rows, EP, split_axis=1, concat_axis=0, tiled=True)
    column_sums = jnp.dot(normed, column_block, preferred_element_type=jnp.float32)
    projected = lax.all_to_all(column_sums, EP, split_axis=0, concat_axis=1, tiled=True)
    query_cols = query_w.shape[1]
    key_cols = key_w.shape[1]
    queries = rotate(
        projected[:, :query_cols].reshape(tok_dev, KV_HEADS, -1, 2, HEAD_DIM),
        lengths[:, None, None, None],
    ).astype(jnp.bfloat16)
    key_new = rotate(
        projected[:, query_cols : query_cols + key_cols].reshape(tok_dev, KV_HEADS, 2, HEAD_DIM),
        lengths[:, None, None],
    ).astype(jnp.bfloat16)
    value_new = projected[:, query_cols + key_cols :].astype(jnp.bfloat16)
    attn_out = attend(
        queries, key_new, value_new, key_cache, value_cache, lengths, lam_heads, head_gain
    )
    pieces = lax.all_to_all(attn_out, EP, split_axis=1, concat_axis=0, tiled=True)
    routed_here = jnp.sum((routing == device).astype(jnp.int32), axis=1)
    attn_proj = summed_rows(
        jnp.dot(pieces, out_w, preferred_element_type=jnp.float32).astype(jnp.bfloat16),
        (("ep_0", "ep_1", "ep_2"), "ep_3"),
        0,
    ).astype(jnp.bfloat16)
    after_mixer = (hidden_in.astype(jnp.float32) + attn_proj.astype(jnp.float32)).astype(
        jnp.bfloat16
    )
    moe_in = rms_scale(after_mixer, moe_gain, eps_norm).astype(jnp.bfloat16)
    own_routes = lax.dynamic_slice_in_dim(routing, device * tok_dev, tok_dev, 0)
    own_weights = lax.dynamic_slice_in_dim(route_weight, device * tok_dev, tok_dev, 0)
    expert_ids = jnp.arange(devices, dtype=jnp.int32)
    matches = own_routes[:, :, None] == expert_ids[None, None, :]
    chosen = jnp.any(matches, axis=1)
    weight_grid = jnp.sum(jnp.where(matches, own_weights[:, :, None], 0.0), axis=1)
    outgoing = jnp.where(chosen.T[:, :, None], moe_in[None], jnp.zeros((), jnp.bfloat16))
    arrived = lax.all_to_all(outgoing, EP, split_axis=0, concat_axis=0, tiled=True)
    result = expert_rows(
        arrived.reshape(devices * tok_dev, model_width), routed_here, gate_w[0], up_w[0], down_w[0]
    ).astype(jnp.bfloat16)
    returned = lax.all_to_all(
        result.reshape(devices, tok_dev, model_width), EP, split_axis=0, concat_axis=0, tiled=True
    )
    routed = jnp.sum(returned.astype(jnp.float32) * weight_grid.T[:, :, None], axis=0)
    shared_hidden = (
        jax.nn.silu(jnp.dot(moe_in, shared_gate, preferred_element_type=jnp.float32))
        * jnp.dot(moe_in, shared_up, preferred_element_type=jnp.float32)
    ).astype(jnp.bfloat16)
    shared_out = jnp.dot(shared_hidden, shared_down, preferred_element_type=jnp.float32)
    layer_out = (after_mixer.astype(jnp.float32) + routed + shared_out).astype(jnp.bfloat16)
    return (layer_out, key_new.reshape(tok_dev, -1), value_new)


def solution(mesh):
    torus = Mesh(mesh.devices.reshape(4, 4, 4, 2), ("ep_0", "ep_1", "ep_2", "ep_3"))
    return jax.shard_map(
        on_device,
        mesh=torus,
        in_specs=(
            P(EP, None),
            P(EP),
            P(EP, None, None),
            P(EP, None, None),
            P(EP, None),
            P(EP, None),
            P(EP, None),
            P(EP, None),
            P(),
            P(),
            P(),
            P(),
            P(),
            P(),
            P(EP, None, None),
            P(EP, None, None),
            P(EP, None, None),
            P(),
            P(),
            P(),
        ),
        out_specs=(P(EP, None), P(EP, None), P(EP, None)),
        check_vma=False,
    )
```

profile of v0, /device:TPU:1, one launch (start us, length us, event | category | flops | bytes accessed | tf_op | source)
XLA Modules:
  0.0 221.3 jit_solution(17257553948698546519)
XLA Ops:
  10.0 1.2 reshape.270
  11.2 11.5 %all-to-all-start = ((bf16[128,2,192]{2,1,0:T(2,128)(2,1)}), bf16[128,2,192]{2,1,0:T(2,128)(2,1)S(1)}, u32[]{:S(2)}, u32[]{:S(2)}) async-start(bf16[128,2,192]{2,1,0:T(2,128)(2,1)} %reshape.270), calls=%async_computation | async-start | bytes 262144 | tf_op jit(solution)/shard_map/all_to_all | solution.py:145
  22.8 9.9 %all-to-all-done = bf16[128,2,192]{2,1,0:T(2,128)(2,1)S(1)} async-done(((bf16[128,2,192]{2,1,0:T(2,128)(2,1)}), bf16[128,2,192]{2,1,0:T(2,128)(2,1)S(1)}, u32[]{:S(2)}, u32[]{:S(2)}) %all-to-all-start) | async-done | bytes 98336 | tf_op jit(solution)/shard_map/all_to_all | solution.py:145
  32.7 1.2 reshape.271
  33.9 44.1 %all-gather.3.cloned.1.call-done = bf16[128,2,2048]{2,1,0:T(2,128)(2,1)} async-done(((bf16[1,2,2048]{2,1,0:T(2,128)(2,1)}), bf16[128,2,2048]{2,1,0:T(2,128)(2,1)}) %all-gather.3.cloned.1.call-update) | async-done | bytes 1048592 | tf_op jit(solution)/shard_map/all_gather | solution.py:142
  78.0 2.5 %reshape.265 = f32[256,2048]{1,0:T(8,128)} reshape(bf16[128,2,2048]{2,1,0:T(2,128)(2,1)} %all-gather.3.cloned.1.call-done) | data formatting | bytes 3145728 | tf_op jit(solution)/shard_map/convert_element_type | solution.py:39
  80.6 2.0 multiply_reduce_fusion.1
  83.0 1.5 dot_general.41
  84.5 2.1 fusion.29
  87.4 5.4 %all-to-all-start.1 = ((f32[128,2,24]{2,1,0:T(2,128)}), f32[128,2,24]{2,1,0:T(2,128)S(1)}, u32[]{:S(2)}, u32[]{:S(2)}) async-start(f32[128,2,24]{2,1,0:T(2,128)} %copy.77), calls=%async_computation.1 | async-start | bytes 262144 | tf_op jit(solution)/shard_map/all_to_all | solution.py:147
  92.9 4.0 %reshape.254 = bf16[2,1024,2,2,128]{4,3,2,1,0:T(2,128)(2,1)} reshape(bf16[2,1024,512]{2,1,0:T(8,128)(2,1)} %param.22) | data formatting | bytes 4194304 | tf_op jit(solution)/shard_map/reshape | solution.py:66
  96.9 5.8 %all-to-all-done.1 = f32[128,2,24]{2,1,0:T(2,128)S(1)} async-done(((f32[128,2,24]{2,1,0:T(2,128)}), f32[128,2,24]{2,1,0:T(2,128)S(1)}, u32[]{:S(2)}, u32[]{:S(2)}) %all-to-all-start.1) | async-done | bytes 24608 | tf_op jit(solution)/shard_map/all_to_all | solution.py:147
  103.5 2.4 %select_reduce_fusion = (f32[2,2,4,2]{2,3,1,0:T(2,128)S(1)}, f32[2,2,4,2,1024]{4,2,3,1,0:T(4,128)S(1)}) fusion(pred[2,1024]{1,0:T(4,128)(4,1)S(1)} %iota_compare_fusion.1, bf16[2,1024,2,2,128]{4,3,2,1,0:T(2,128)(2,1)} %reshape.254, bf16[2,2,4,2,64]{4,2,3,1,0:T(4,128)(2,1)S(1)} %get-tuple-element.8, bf16[2,2,4,2,64]{4,2,3,1,0:T(4,128)(2,1)S(1)} %get-tuple-element.7), kind=kOutput, calls=%fused_computation.31 | convolution fusion | flops 8503264 | bytes 2238592 | tf_op jit(solution)/shard_map/skgph,sckph->skgpc/dot_general | solution.py:71
  106.1 2.1 multiply_reduce_fusion.2
  108.5 13.7 %all_to_all.74 = bf16[2,128,16]{2,0,1:T(2,128)(2,1)S(1)} all-to-all(bf16[2,128,16]{2,0,1:T(2,128)(2,1)S(1)} %copy.84), channel_id=1, replica_groups=mesh['ep_0'=4,'ep_1'=4,'ep_2'=4,'ep_3'=2] {'ep_0','ep_1','ep_2','ep_3'}, dimensions={1} | all-to-all | bytes 16384 | tf_op jit(solution)/shard_map/all_to_all | solution.py:162
  122.6 1.5 reshape_reshape.3
  124.1 1.9 copy.125
  126.0 5.0 %all_to_all.75 = bf16[2,64,2,2048]{3,2,1,0:T(2,128)(2,1)S(1)} all-to-all(bf16[2,64,2,2048]{3,2,1,0:T(2,128)(2,1)S(1)} %bitcast.97), channel_id=1, replica_groups=mesh['ep_0'=4,'ep_1'=4,'ep_2'=4,'ep_3'=2] {'ep_3'}, dimensions={0} | all-to-all | bytes 2097152 | tf_op jit(solution)/shard_map/all_to_all | solution.py:24
  131.0 3.1 %reduce_sum.90 = bf16[64,2,2048]{2,1,0:T(2,128)(2,1)} reduce(bf16[2,64,2,2048]{3,2,1,0:T(2,128)(2,1)S(1)} %all_to_all.75, bf16[]{:T(256)} %constant.30.clone.1), dimensions={0}, to_apply=%region_4.5 | reduce | flops 262144 | bytes 1572866 | tf_op jit(solution)/shard_map/reduce_sum | solution.py:25
  134.1 4.9 %all-to-all-start.4 = ((bf16[64,2,2048]{2,1,0:T(2,128)(2,1)}), bf16[64,2,2048]{2,1,0:T(2,128)(2,1)S(1)}, u32[]{:S(2)}, u32[]{:S(2)}) async-start(bf16[64,2,2048]{2,1,0:T(2,128)(2,1)} %reduce_sum.90), calls=%async_computation.4 | async-start | bytes 1048576 | tf_op jit(solution)/shard_map/all_to_all | solution.py:32
  139.3 12.1 %all-to-all-done.4 = bf16[64,2,2048]{2,1,0:T(2,128)(2,1)S(1)} async-done(((bf16[64,2,2048]{2,1,0:T(2,128)(2,1)}), bf16[64,2,2048]{2,1,0:T(2,128)(2,1)S(1)}, u32[]{:S(2)}, u32[]{:S(2)}) %all-to-all-start.4) | async-done | bytes 524320 | tf_op jit(solution)/shard_map/all_to_all | solution.py:32
  152.1 1.8 broadcast_select_fusion
  153.9 5.3 %all-to-all-start.5 = ((bf16[128,2,2048]{2,1,0:T(2,128)(2,1)}), bf16[128,2,2048]{2,1,0:T(2,128)(2,1)S(1)}, u32[]{:S(2)}, u32[]{:S(2)}) async-start(bf16[128,2,2048]{2,1,0:T(2,128)(2,1)} %broadcast_select_fusion), calls=%async_computation.5 | async-start | bytes 2097152 | tf_op jit(solution)/shard_map/all_to_all | solution.py:180
  159.8 18.7 %all-to-all-done.5 = bf16[128,2,2048]{2,1,0:T(2,128)(2,1)S(1)} async-done(((bf16[128,2,2048]{2,1,0:T(2,128)(2,1)}), bf16[128,2,2048]{2,1,0:T(2,128)(2,1)S(1)}, u32[]{:S(2)}, u32[]{:S(2)}) %all-to-all-start.5) | async-done | bytes 1048608 | tf_op jit(solution)/shard_map/all_to_all | solution.py:180
  178.6 1.2 reshape.259
  179.8 1.6 convolution_convert_fusion.3
  181.4 2.0 fusion.7
  184.5 1.5 reshape.260
  186.0 4.4 %all-to-all-start.6 = ((bf16[128,2,2048]{2,1,0:T(2,128)(2,1)}), bf16[128,2,2048]{2,1,0:T(2,128)(2,1)S(1)}, u32[]{:S(2)}, u32[]{:S(2)}) async-start(bf16[128,2,2048]{2,1,0:T(2,128)(2,1)} %reshape.260), calls=%async_computation.6 | async-start | bytes 2097152 | tf_op jit(solution)/shard_map/all_to_all | solution.py:184
  191.4 2.0 fusion.62
  193.4 16.4 %all-to-all-done.6 = bf16[128,2,2048]{2,1,0:T(2,128)(2,1)S(1)} async-done(((bf16[128,2,2048]{2,1,0:T(2,128)(2,1)}), bf16[128,2,2048]{2,1,0:T(2,128)(2,1)S(1)}, u32[]{:S(2)}, u32[]{:S(2)}) %all-to-all-start.6) | async-done | bytes 1048608 | tf_op jit(solution)/shard_map/all_to_all | solution.py:184
  210.9 3.6 %fusion = bf16[2,2048]{1,0:T(2,128)(2,1)} fusion(bf16[512,2048]{1,0:T(8,128)(2,1)} %param.39, bf16[2,2048]{1,0:T(2,128)(2,1)S(1)} %fusion.42, bf16[2048,512]{1,0:T(8,128)(2,1)} %param.38, f32[2,2048]{1,0:T(2,128)S(1)} %multiply_reduce_fusion, f32[2,512]{1,0:T(2,128)S(1)} %fusion.62, bf16[2,2048]{1,0:T(2,128)(2,1)S(1)} %reduce_sum.91, ...), kind=kOutput, calls=%fused_computation.5 | convolution fusion | flops 8427520 | bytes 4247552 | tf_op jit(solution)/shard_map/dot_general | solution.py:192
  (83 shorter events, 10.7 us)
Async XLA Ops:
  7.2 176.6 %copy-start = (bf16[1,512,2048]{2,1,0:T(8,128)(2,1)S(1)}, bf16[1,512,2048]{2,1,0:T(8,128)(2,1)}, u32[]{:S(2)}) copy-start(bf16[1,512,2048]{2,1,0:T(8,128)(2,1)} %param.36) | copy-start | bytes 6291460
  7.2 15.5 %copy-start.11 = (s32[2]{0:T(128)S(1)}, s32[2]{0:T(128)}, u32[]{:S(2)}) copy-start(s32[2]{0:T(128)} %param.21) | copy-start | bytes 28
  7.2 70.8 %all-gather.3.cloned.1.call-start = ((), (), s32[]{:S(2)}) async-start(), calls=%async_computation.7 | async-start | bytes 1056768 | tf_op jit(solution)/shard_map/all_gather | solution.py:142
  11.2 21.5 %all-to-all-start = ((bf16[128,2,192]{2,1,0:T(2,128)(2,1)}), bf16[128,2,192]{2,1,0:T(2,128)(2,1)S(1)}, u32[]{:S(2)}, u32[]{:S(2)}) async-start(bf16[128,2,192]{2,1,0:T(2,128)(2,1)} %reshape.270), calls=%async_computation | async-start | bytes 262144 | tf_op jit(solution)/shard_map/all_to_all | solution.py:145
  33.9 48.7 %copy-start.6 = (f32[2048]{0:T(1024)S(1)}, f32[2048]{0:T(1024)}, u32[]{:S(2)}) copy-start(f32[2048]{0:T(1024)} %param.30) | copy-start | bytes 24580
  80.6 2.2 %copy-start.1 = (f32[256,2048]{1,0:T(8,128)S(1)}, f32[256,2048]{1,0:T(8,128)}, u32[]{:S(2)}) copy-start(f32[256,2048]{1,0:T(8,128)} %reshape.265) | copy-start | bytes 6291460
  87.4 15.4 %all-to-all-start.1 = ((f32[128,2,24]{2,1,0:T(2,128)}), f32[128,2,24]{2,1,0:T(2,128)S(1)}, u32[]{:S(2)}, u32[]{:S(2)}) async-start(f32[128,2,24]{2,1,0:T(2,128)} %copy.77), calls=%async_computation.1 | async-start | bytes 262144 | tf_op jit(solution)/shard_map/all_to_all | solution.py:147
  92.9 4.0 %copy-start.12 = (f32[8]{0:T(128)S(1)}, f32[8]{0:T(128)}, u32[]{:S(2)}) copy-start(f32[8]{0:T(128)} %param.28) | copy-start | bytes 100
  102.9 5.3 %copy-start.7 = (bf16[2,512]{1,0:T(2,128)(2,1)}, bf16[2,512]{1,0:T(2,128)(2,1)S(1)}, u32[]{:S(2)}) copy-start(bf16[2,512]{1,0:T(2,128)(2,1)S(1)} %slice.111) | copy-start | bytes 6148
  105.8 2.4 %copy-start.10 = (f32[256]{0:T(256)S(1)}, f32[256]{0:T(256)}, u32[]{:S(2)}) copy-start(f32[256]{0:T(256)} %param.29) | copy-start | bytes 3076
  105.8 16.3 %copy-start.4 = (bf16[16,2048]{1,0:T(8,128)(2,1)S(1)}, bf16[16,2048]{1,0:T(8,128)(2,1)}, u32[]{:S(2)}) copy-start(bf16[16,2048]{1,0:T(8,128)(2,1)} %param.27) | copy-start | bytes 196612
  126.0 13.0 %copy-start.5 = (s32[256,6]{0,1:T(8,128)S(1)}, s32[256,6]{0,1:T(8,128)}, u32[]{:S(2)}) copy-start(s32[256,6]{0,1:T(8,128)} %param.32) | copy-start | bytes 18436
  131.0 20.9 %copy-start.3 = (bf16[2,2048]{1,0:T(2,128)(2,1)S(1)}, bf16[2,2048]{1,0:T(2,128)(2,1)}, u32[]{:S(2)}) copy-start(bf16[2,2048]{1,0:T(2,128)(2,1)} %param.20) | copy-start | bytes 24580
  131.0 21.0 %copy-start.8 = (f32[2048]{0:T(1024)S(1)}, f32[2048]{0:T(1024)}, u32[]{:S(2)}) copy-start(f32[2048]{0:T(1024)} %param.31) | copy-start | bytes 24580
  134.1 17.3 %all-to-all-start.4 = ((bf16[64,2,2048]{2,1,0:T(2,128)(2,1)}), bf16[64,2,2048]{2,1,0:T(2,128)(2,1)S(1)}, u32[]{:S(2)}, u32[]{:S(2)}) async-start(bf16[64,2,2048]{2,1,0:T(2,128)(2,1)} %reduce_sum.90), calls=%async_computation.4 | async-start | bytes 1048576 | tf_op jit(solution)/shard_map/all_to_all | solution.py:32
  153.9 24.7 %all-to-all-start.5 = ((bf16[128,2,2048]{2,1,0:T(2,128)(2,1)}), bf16[128,2,2048]{2,1,0:T(2,128)(2,1)S(1)}, u32[]{:S(2)}, u32[]{:S(2)}) async-start(bf16[128,2,2048]{2,1,0:T(2,128)(2,1)} %broadcast_select_fusion), calls=%async_computation.5 | async-start | bytes 2097152 | tf_op jit(solution)/shard_map/all_to_all | solution.py:180
  179.8 3.6 %copy-start.2 = (bf16[1,2048,512]{2,1,0:T(8,128)(2,1)S(1)}, bf16[1,2048,512]{2,1,0:T(8,128)(2,1)}, u32[]{:S(2)}) copy-start(bf16[1,2048,512]{2,1,0:T(8,128)(2,1)} %param.35) | copy-start | bytes 6291460
  184.5 6.0 %copy-start.9 = (f32[256,6]{0,1:T(8,128)S(1)}, f32[256,6]{0,1:T(8,128)}, u32[]{:S(2)}) copy-start(f32[256,6]{0,1:T(8,128)} %param.33) | copy-start | bytes 18436
  186.0 23.8 %all-to-all-start.6 = ((bf16[128,2,2048]{2,1,0:T(2,128)(2,1)}), bf16[128,2,2048]{2,1,0:T(2,128)(2,1)S(1)}, u32[]{:S(2)}, u32[]{:S(2)}) async-start(bf16[128,2,2048]{2,1,0:T(2,128)(2,1)} %reshape.260), calls=%async_computation.6 | async-start | bytes 2097152 | tf_op jit(solution)/shard_map/all_to_all | solution.py:184
Sparse Core Ops, SparseCore 0:
  10.8 67.1 all-gather.2
where the time goes:
time: 222 us; the launch traced here: 221 us
  waiting for transfers between devices  108 us (49%)
  starting transfers between devices  31.5 us (14%)
  local copies, waits for them, and re-layouts  20.6 us (9%)
  blocking collectives  18.6 us (8%)
  matrix products  17.3 us (8%)
  between operations  14.3 us (6%)
  other arithmetic  11.2 us (5%)
    all_gather x1, waiting for transfers between devices, on_device(): all_rows = lax.all_gather(hidden_in, EP, axis=0, tiled=True)  44.1 us
    all_to_all x1, waiting for transfers between devices, on_device(): lax.all_to_all(outgoing, EP, split_axis=0, concat_axis=0, tiled=True)  18.7 us
    all_to_all x1, waiting for transfers between devices, on_device(): lax.all_to_all(result.reshape(devices, tok_dev, model_width), EP, split_a...  16.4 us
    all_to_all x1, blocking collectives, on_device(): lax.all_to_all(attn_out, EP, split_axis=1, concat_axis=0, tiled=True)  13.7 us
    all_to_all x1, waiting for transfers between devices, summed_rows(): lax.all_to_all(nearer.astype(jnp.bfloat16), far, split_axis=0, concat_axi...  12.1 us
    all_to_all x1, starting transfers between devices, on_device(): lax.all_to_all(joined_rows, EP, split_axis=1, concat_axis=0, tiled=True)  11.5 us
    all_to_all x1, waiting for transfers between devices, on_device(): lax.all_to_all(joined_rows, EP, split_axis=1, concat_axis=0, tiled=True)  9.9 us
    all_to_all x1, waiting for transfers between devices, on_device(): lax.all_to_all(column_sums, EP, split_axis=0, concat_axis=1, tiled=True)  5.83 us
  transfers between devices with their start and end apart: 6, of which 6 were waited for; matrix products, arithmetic and copies ran while one was open for 5% of the time, Pallas kernels for 0%

commit v1 on v0

--- a/solution.py
+++ b/solution.py
@@ -139,7 +139,9 @@
     device = lax.axis_index(EP)
     tok_dev = hidden_in.shape[0]
     model_width = hidden_in.shape[1]
-    all_rows = lax.all_gather(hidden_in, EP, axis=0, tiled=True)
+    all_rows = jnp.concatenate(
+        lax.all_to_all(jnp.stack([hidden_in] * lax.axis_size(EP)), EP, 0, 0), axis=0
+    )
     normed = rms_scale(all_rows, attn_gain, eps_norm).astype(jnp.bfloat16)
     joined_rows = jnp.concatenate([query_w, key_w, value_w], axis=1)
     column_block = lax.all_to_all(joined_rows, EP, split_axis=1, concat_axis=0, tiled=True)

time: 222 us -> 180 us (0.81)
  waiting for transfers between devices: 108 us -> 71.1 us
  blocking collectives: 18.6 us -> 40.1 us
  between operations: 14.3 us -> 0.95 us
  starting transfers between devices: 31.5 us -> 23.3 us
  local copies, waits for them, and re-layouts: 20.6 us -> 17.2 us
    all_gather x1 -> x0, waiting for transfers between devices: 44.1 us -> none  [on_device(): all_rows = lax.all_gather(hidden_in, EP, axis=0, tiled=True)]
    all_to_all x0 -> x1, blocking collectives: none -> 21.4 us  [on_device(): lax.all_to_all(joined_rows, EP, split_axis=1, concat_axis=0, tiled=True)]
    all_to_all x1, waiting for transfers between devices: 9.9 us -> 17.9 us  [on_device(): lax.all_to_all(jnp.stack([hidden_in] * lax.axis_size(EP)), EP, 0, 0)]
    all_to_all x1, starting transfers between devices: 11.5 us -> 4.32 us  [on_device(): lax.all_to_all(jnp.stack([hidden_in] * lax.axis_size(EP)), EP, 0, 0)]
    convert_element_type x1 -> x0, local copies, waits for them, and re-layouts: 2.54 us -> none  [rms_scale(): row_block = row_block.astype(jnp.float32)]
  transfers between devices with their start and end apart: 6 -> 5, of which waited for: 6 -> 5; matrix products, arithmetic and copies ran while one was open for 5% -> 5% of each run, Pallas kernels for 0% -> 0%
where the time goes in v1:
time: 180 us; the launch traced here: 179 us
  waiting for transfers between devices  71.1 us (39%)
  blocking collectives  40.1 us (22%)
  starting transfers between devices  23.3 us (13%)
  local copies, waits for them, and re-layouts  17.2 us (10%)
  matrix products  17.1 us (10%)
  other arithmetic  9.54 us (5%)
    all_to_all x1, blocking collectives, on_device(): lax.all_to_all(joined_rows, EP, split_axis=1, concat_axis=0, tiled=True)  21.4 us
    all_to_all x1, waiting for transfers between devices, on_device(): lax.all_to_all(outgoing, EP, split_axis=0, concat_axis=0, tiled=True)  18.7 us
    all_to_all x1, waiting for transfers between devices, on_device(): lax.all_to_all(jnp.stack([hidden_in] * lax.axis_size(EP)), EP, 0, 0)  17.9 us
    all_to_all x1, waiting for transfers between devices, on_device(): lax.all_to_all(result.reshape(devices, tok_dev, model_width), EP, split_a...  16.4 us
    all_to_all x1, blocking collectives, on_device(): lax.all_to_all(attn_out, EP, split_axis=1, concat_axis=0, tiled=True)  13.7 us
    all_to_all x1, waiting for transfers between devices, summed_rows(): lax.all_to_all(nearer.astype(jnp.bfloat16), far, split_axis=0, concat_axi...  12.2 us
    all_to_all x1, waiting for transfers between devices, on_device(): lax.all_to_all(column_sums, EP, split_axis=0, concat_axis=1, tiled=True)  5.92 us
    all_to_all x1, starting transfers between devices, on_device(): lax.all_to_all(outgoing, EP, split_axis=0, concat_axis=0, tiled=True)  5.21 us
  transfers between devices with their start and end apart: 5, of which 5 were waited for; matrix products, arithmetic and copies ran while one was open for 5% of the time, Pallas kernels for 0%

profile of v1, /device:TPU:1, one launch (start us, length us, event | category | flops | bytes accessed | tf_op | source)
XLA Modules:
  0.0 179.2 jit_solution(14020904073159830725)
XLA Ops:
  0.7 1.0 pad_maximum_fusion
  1.7 0.8 all_to_all.56
  3.4 21.4 %all_to_all.79 = bf16[128,2,192]{2,1,0:T(2,128)(2,1)S(1)} all-to-all(bf16[128,2,192]{2,1,0:T(2,128)(2,1)S(1)} %reshape.283), channel_id=1, replica_groups=mesh['ep_0'=4,'ep_1'=4,'ep_2'=4,'ep_3'=2] {'ep_0','ep_1','ep_2','ep_3'}, dimensions={0} | all-to-all | bytes 196608 | tf_op jit(solution)/shard_map/all_to_all | solution.py:147
  24.9 1.5 stack.2
  26.4 4.3 %all-to-all-start = ((bf16[128,2,2048]{2,1,0:T(2,128)(2,1)}), bf16[128,2,2048]{2,1,0:T(2,128)(2,1)S(1)}, u32[]{:S(2)}, u32[]{:S(2)}) async-start(bf16[128,2,2048]{2,1,0:T(2,128)(2,1)} %stack.2), calls=%async_computation | async-start | bytes 2097152 | tf_op jit(solution)/shard_map/all_to_all | solution.py:143
  30.8 1.2 reshape.284
  32.1 17.9 %all-to-all-done = bf16[128,2,2048]{2,1,0:T(2,128)(2,1)S(1)} async-done(((bf16[128,2,2048]{2,1,0:T(2,128)(2,1)}), bf16[128,2,2048]{2,1,0:T(2,128)(2,1)S(1)}, u32[]{:S(2)}, u32[]{:S(2)}) %all-to-all-start) | async-done | bytes 1048608 | tf_op jit(solution)/shard_map/all_to_all | solution.py:143
  50.4 1.8 fusion.32
  52.9 4.4 %all-to-all-start.2 = ((f32[128,2,24]{2,1,0:T(2,128)}), f32[128,2,24]{2,1,0:T(2,128)S(1)}, u32[]{:S(2)}, u32[]{:S(2)}) async-start(f32[128,2,24]{2,1,0:T(2,128)} %copy.92), calls=%async_computation.2 | async-start | bytes 262144 | tf_op jit(solution)/shard_map/all_to_all | solution.py:149
  57.5 4.0 %reshape.270 = bf16[2,1024,2,2,128]{4,3,2,1,0:T(2,128)(2,1)} reshape(bf16[2,1024,512]{2,1,0:T(8,128)(2,1)} %param.22) | data formatting | bytes 4194304 | tf_op jit(solution)/shard_map/reshape | solution.py:66
  61.5 5.9 %all-to-all-done.2 = f32[128,2,24]{2,1,0:T(2,128)S(1)} async-done(((f32[128,2,24]{2,1,0:T(2,128)}), f32[128,2,24]{2,1,0:T(2,128)S(1)}, u32[]{:S(2)}, u32[]{:S(2)}) %all-to-all-start.2) | async-done | bytes 24608 | tf_op jit(solution)/shard_map/all_to_all | solution.py:149
  68.1 2.4 %select_reduce_fusion = (f32[2,2,4,2]{2,3,1,0:T(2,128)S(1)}, f32[2,2,4,2,1024]{4,2,3,1,0:T(4,128)S(1)}) fusion(pred[2,1024]{1,0:T(4,128)(4,1)S(1)} %iota_compare_fusion.1, bf16[2,1024,2,2,128]{4,3,2,1,0:T(2,128)(2,1)} %reshape.270, bf16[2,2,4,2,64]{4,2,3,1,0:T(4,128)(2,1)S(1)} %get-tuple-element.8, bf16[2,2,4,2,64]{4,2,3,1,0:T(4,128)(2,1)S(1)} %get-tuple-element.7), kind=kOutput, calls=%fused_computation.36 | convolution fusion | flops 8503264 | bytes 2238592 | tf_op jit(solution)/shard_map/skgph,sckph->skgpc/dot_general | solution.py:71
  70.8 2.1 %multiply_reduce_fusion.1 = (f32[2,2,4]{2,1,0:T(2,128)S(1)}, f32[2,2,4,256]{3,2,1,0:T(4,128)S(1)}) fusion(f32[2,2,256]{2,1,0:T(2,128)S(1)} %reshape.278, f32[2,2,4]{2,1,0:T(2,128)S(1)} %bitcast.105, bf16[2,128,2,8,256]{4,3,2,1,0:T(8,128)(2,1)} %bitcast.109, f32[2,2,4,2,1024]{4,2,3,1,0:T(4,128)S(1)} %get-tuple-element.6, f32[2,2,4]{2,1,0:T(2,128)S(1)} %bitcast.106, ...), kind=kOutput, calls=%fused_computation.56 | convolution fusion | flops 8486896 | bytes 2248992 | tf_op jit(solution)/shard_map/skgc,sckv->skgv/dot_general | solution.py:91
  73.2 13.7 %all_to_all.80 = bf16[2,128,16]{2,0,1:T(2,128)(2,1)S(1)} all-to-all(bf16[2,128,16]{2,0,1:T(2,128)(2,1)S(1)} %copy.99), channel_id=1, replica_groups=mesh['ep_0'=4,'ep_1'=4,'ep_2'=4,'ep_3'=2] {'ep_0','ep_1','ep_2','ep_3'}, dimensions={1} | all-to-all | bytes 16384 | tf_op jit(solution)/shard_map/all_to_all | solution.py:164
  87.2 1.5 reshape_reshape.3
  88.8 1.9 %copy.143 = bf16[64,2,2,2048]{3,2,0,1:T(2,128)(2,1)S(1)} copy(bf16[64,2,2,2048]{3,2,1,0:T(2,128)(2,1)} %reshape_reshape.3) | data formatting | bytes 2097152 | tf_op jit(solution)/shard_map/reshape;reshape | solution.py:18
  90.7 5.0 %all_to_all.81 = bf16[2,64,2,2048]{3,2,1,0:T(2,128)(2,1)S(1)} all-to-all(bf16[2,64,2,2048]{3,2,1,0:T(2,128)(2,1)S(1)} %bitcast.96), channel_id=1, replica_groups=mesh['ep_0'=4,'ep_1'=4,'ep_2'=4,'ep_3'=2] {'ep_3'}, dimensions={0} | all-to-all | bytes 2097152 | tf_op jit(solution)/shard_map/all_to_all | solution.py:24
  95.7 3.1 %reduce_sum.90 = bf16[64,2,2048]{2,1,0:T(2,128)(2,1)} reduce(bf16[2,64,2,2048]{3,2,1,0:T(2,128)(2,1)S(1)} %all_to_all.81, bf16[]{:T(256)} %constant.30.clone.1), dimensions={0}, to_apply=%region_4.5 | reduce | flops 262144 | bytes 1572866 | tf_op jit(solution)/shard_map/reduce_sum | solution.py:25
  98.8 4.9 %all-to-all-start.5 = ((bf16[64,2,2048]{2,1,0:T(2,128)(2,1)}), bf16[64,2,2048]{2,1,0:T(2,128)(2,1)S(1)}, u32[]{:S(2)}, u32[]{:S(2)}) async-start(bf16[64,2,2048]{2,1,0:T(2,128)(2,1)} %reduce_sum.90), calls=%async_computation.5 | async-start | bytes 1048576 | tf_op jit(solution)/shard_map/all_to_all | solution.py:32
  104.0 12.2 %all-to-all-done.5 = bf16[64,2,2048]{2,1,0:T(2,128)(2,1)S(1)} async-done(((bf16[64,2,2048]{2,1,0:T(2,128)(2,1)}), bf16[64,2,2048]{2,1,0:T(2,128)(2,1)S(1)}, u32[]{:S(2)}, u32[]{:S(2)}) %all-to-all-start.5) | async-done | bytes 524320 | tf_op jit(solution)/shard_map/all_to_all | solution.py:32
  116.9 1.8 %broadcast_select_fusion = bf16[128,2,2048]{2,1,0:T(2,128)(2,1)} fusion(pred[128,2]{1,0:T(8,128)(4,1)S(1)} %copy.103, bf16[2,2048]{1,0:T(2,128)(2,1)S(1)} %fusion.48), kind=kLoop, calls=%fused_computation.22 | loop fusion | flops 524288 | bytes 1057024 | tf_op jit(solution)/shard_map/jit(_where)/select_n | solution.py:181
  118.7 5.2 %all-to-all-start.6 = ((bf16[128,2,2048]{2,1,0:T(2,128)(2,1)}), bf16[128,2,2048]{2,1,0:T(2,128)(2,1)S(1)}, u32[]{:S(2)}, u32[]{:S(2)}) async-start(bf16[128,2,2048]{2,1,0:T(2,128)(2,1)} %broadcast_select_fusion), calls=%async_computation.6 | async-start | bytes 2097152 | tf_op jit(solution)/shard_map/all_to_all | solution.py:182
  124.6 18.7 %all-to-all-done.6 = bf16[128,2,2048]{2,1,0:T(2,128)(2,1)S(1)} async-done(((bf16[128,2,2048]{2,1,0:T(2,128)(2,1)}), bf16[128,2,2048]{2,1,0:T(2,128)(2,1)S(1)}, u32[]{:S(2)}, u32[]{:S(2)}) %all-to-all-start.6) | async-done | bytes 1048608 | tf_op jit(solution)/shard_map/all_to_all | solution.py:182
  143.3 1.2 reshape.275
  144.5 1.6 convolution_convert_fusion.3
  146.1 2.0 %fusion.10 = f32[24,512]{1,0:T(8,128)S(1)} fusion(bf16[24,2048]{1,0:T(8,128)(2,1)S(1)} %convolution_convert_fusion.3, bf16[1,2048,512]{2,1,0:T(8,128)(2,1)} %param.34), kind=kOutput, calls=%fused_computation.17 | convolution fusion | flops 50331648 | bytes 2244608 | tf_op jit(solution)/shard_map/dot_general | solution.py:109
  149.2 1.5 reshape.276
  150.8 4.4 %all-to-all-start.7 = ((bf16[128,2,2048]{2,1,0:T(2,128)(2,1)}), bf16[128,2,2048]{2,1,0:T(2,128)(2,1)S(1)}, u32[]{:S(2)}, u32[]{:S(2)}) async-start(bf16[128,2,2048]{2,1,0:T(2,128)(2,1)} %reshape.276), calls=%async_computation.7 | async-start | bytes 2097152 | tf_op jit(solution)/shard_map/all_to_all | solution.py:186
  156.2 2.0 %fusion.68 = f32[2,512]{1,0:T(2,128)S(1)} fusion(bf16[2,2048]{1,0:T(2,128)(2,1)S(1)} %fusion.48, bf16[2048,512]{1,0:T(8,128)(2,1)} %param.37), kind=kOutput, calls=%fused_computation.104 | convolution fusion | flops 4194304 | bytes 2109440 | tf_op jit(solution)/shard_map/dot_general | solution.py:191
  158.1 16.4 %all-to-all-done.7 = bf16[128,2,2048]{2,1,0:T(2,128)(2,1)S(1)} async-done(((bf16[128,2,2048]{2,1,0:T(2,128)(2,1)}), bf16[128,2,2048]{2,1,0:T(2,128)(2,1)S(1)}, u32[]{:S(2)}, u32[]{:S(2)}) %all-to-all-start.7) | async-done | bytes 1048608 | tf_op jit(solution)/shard_map/all_to_all | solution.py:186
  174.5 1.1 multiply_reduce_fusion
  175.7 3.6 %fusion = bf16[2,2048]{1,0:T(2,128)(2,1)} fusion(bf16[512,2048]{1,0:T(8,128)(2,1)} %param.39, bf16[2,2048]{1,0:T(2,128)(2,1)S(1)} %fusion.48, bf16[2048,512]{1,0:T(8,128)(2,1)} %param.38, f32[2,2048]{1,0:T(2,128)S(1)} %multiply_reduce_fusion, f32[2,512]{1,0:T(2,128)S(1)} %fusion.68, bf16[2,2048]{1,0:T(2,128)(2,1)S(1)} %reduce_sum.91, ...), kind=kOutput, calls=%fused_computation.7 | convolution fusion | flops 8427520 | bytes 4247552 | tf_op jit(solution)/shard_map/dot_general | solution.py:194
  (77 shorter events, 7.6 us)
Async XLA Ops:
  0.6 147.9 %copy-start = (bf16[1,512,2048]{2,1,0:T(8,128)(2,1)S(1)}, bf16[1,512,2048]{2,1,0:T(8,128)(2,1)}, u32[]{:S(2)}) copy-start(bf16[1,512,2048]{2,1,0:T(8,128)(2,1)} %param.36) | copy-start | bytes 6291460
  0.6 24.2 %copy-start.2 = (bf16[2,2048]{1,0:T(2,128)(2,1)S(1)}, bf16[2,2048]{1,0:T(2,128)(2,1)}, u32[]{:S(2)}) copy-start(bf16[2,2048]{1,0:T(2,128)(2,1)} %param.20) | copy-start | bytes 24580
  2.9 27.9 %copy-start.9 = (s32[2]{0:T(128)S(1)}, s32[2]{0:T(128)}, u32[]{:S(2)}) copy-start(s32[2]{0:T(128)} %param.21) | copy-start | bytes 28
  26.4 24.0 %copy-start.10 = (f32[2048]{0:T(1024)S(1)}, f32[2048]{0:T(1024)}, u32[]{:S(2)}) copy-start(f32[2048]{0:T(1024)} %param.30) | copy-start | bytes 24580
  26.4 23.6 %all-to-all-start = ((bf16[128,2,2048]{2,1,0:T(2,128)(2,1)}), bf16[128,2,2048]{2,1,0:T(2,128)(2,1)S(1)}, u32[]{:S(2)}, u32[]{:S(2)}) async-start(bf16[128,2,2048]{2,1,0:T(2,128)(2,1)} %stack.2), calls=%async_computation | async-start | bytes 2097152 | tf_op jit(solution)/shard_map/all_to_all | solution.py:143
  52.9 14.5 %all-to-all-start.2 = ((f32[128,2,24]{2,1,0:T(2,128)}), f32[128,2,24]{2,1,0:T(2,128)S(1)}, u32[]{:S(2)}, u32[]{:S(2)}) async-start(f32[128,2,24]{2,1,0:T(2,128)} %copy.92), calls=%async_computation.2 | async-start | bytes 262144 | tf_op jit(solution)/shard_map/all_to_all | solution.py:149
  57.5 4.0 %copy-start.11 = (f32[8]{0:T(128)S(1)}, f32[8]{0:T(128)}, u32[]{:S(2)}) copy-start(f32[8]{0:T(128)} %param.28) | copy-start | bytes 100
  67.6 5.3 %copy-start.5 = (bf16[2,512]{1,0:T(2,128)(2,1)}, bf16[2,512]{1,0:T(2,128)(2,1)S(1)}, u32[]{:S(2)}) copy-start(bf16[2,512]{1,0:T(2,128)(2,1)S(1)} %slice.111) | copy-start | bytes 6148
  70.5 2.4 %copy-start.8 = (f32[256]{0:T(256)S(1)}, f32[256]{0:T(256)}, u32[]{:S(2)}) copy-start(f32[256]{0:T(256)} %param.29) | copy-start | bytes 3076
  70.5 16.3 %copy-start.3 = (bf16[16,2048]{1,0:T(8,128)(2,1)S(1)}, bf16[16,2048]{1,0:T(8,128)(2,1)}, u32[]{:S(2)}) copy-start(bf16[16,2048]{1,0:T(8,128)(2,1)} %param.27) | copy-start | bytes 196612
  90.7 13.0 %copy-start.4 = (s32[256,6]{0,1:T(8,128)S(1)}, s32[256,6]{0,1:T(8,128)}, u32[]{:S(2)}) copy-start(s32[256,6]{0,1:T(8,128)} %param.32) | copy-start | bytes 18436
  95.7 21.1 %copy-start.6 = (f32[2048]{0:T(1024)S(1)}, f32[2048]{0:T(1024)}, u32[]{:S(2)}) copy-start(f32[2048]{0:T(1024)} %param.31) | copy-start | bytes 24580
  98.8 17.4 %all-to-all-start.5 = ((bf16[64,2,2048]{2,1,0:T(2,128)(2,1)}), bf16[64,2,2048]{2,1,0:T(2,128)(2,1)S(1)}, u32[]{:S(2)}, u32[]{:S(2)}) async-start(bf16[64,2,2048]{2,1,0:T(2,128)(2,1)} %reduce_sum.90), calls=%async_computation.5 | async-start | bytes 1048576 | tf_op jit(solution)/shard_map/all_to_all | solution.py:32
  118.7 24.6 %all-to-all-start.6 = ((bf16[128,2,2048]{2,1,0:T(2,128)(2,1)}), bf16[128,2,2048]{2,1,0:T(2,128)(2,1)S(1)}, u32[]{:S(2)}, u32[]{:S(2)}) async-start(bf16[128,2,2048]{2,1,0:T(2,128)(2,1)} %broadcast_select_fusion), calls=%async_computation.6 | async-start | bytes 2097152 | tf_op jit(solution)/shard_map/all_to_all | solution.py:182
  144.5 3.6 %copy-start.1 = (bf16[1,2048,512]{2,1,0:T(8,128)(2,1)S(1)}, bf16[1,2048,512]{2,1,0:T(8,128)(2,1)}, u32[]{:S(2)}) copy-start(bf16[1,2048,512]{2,1,0:T(8,128)(2,1)} %param.35) | copy-start | bytes 6291460
  149.2 6.0 %copy-start.7 = (f32[256,6]{0,1:T(8,128)S(1)}, f32[256,6]{0,1:T(8,128)}, u32[]{:S(2)}) copy-start(f32[256,6]{0,1:T(8,128)} %param.33) | copy-start | bytes 18436
  150.8 23.8 %all-to-all-start.7 = ((bf16[128,2,2048]{2,1,0:T(2,128)(2,1)}), bf16[128,2,2048]{2,1,0:T(2,128)(2,1)S(1)}, u32[]{:S(2)}, u32[]{:S(2)}) async-start(bf16[128,2,2048]{2,1,0:T(2,128)(2,1)} %reshape.276), calls=%async_computation.7 | async-start | bytes 2097152 | tf_op jit(solution)/shard_map/all_to_all | solution.py:186
